TPU v7x, 32 devices: a whole 2x2x4 slice. The times are simulated.
32 devices in a mesh: grp: 2 (over y), fs: 4 (over z), tp: 4 (over x, core).
Axes of the slice: x: 2, y: 2, z: 4, core: 2. Of those that a mesh axis runs over, the one named last changes fastest.
Arguments:
- prompt: bfloat16 [1024, 2048], P(('grp', 'fs', 'tp')), parts along dimension 0, may hold values from -6 to 6
- norm_gain: float32 [2048], P('fs'), may hold values from 0.1 to 1.9
- up_weight: float32 [2048, 8192], P('fs', 'tp'), may hold values from -0.125 to 0.125
- down_weight: float32 [8192, 2048], P('fs', 'tp'), may hold values from -0.0625 to 0.0625
Outputs:
- up_serving: bfloat16 [4096, 8192], P('grp', 'fs'), parts along dimension 0
- down_serving: bfloat16 [8192, 4096], P('fs', 'grp'), parts along dimension 1
- mlp_output: bfloat16 [1024, 2048], P(('grp', 'fs', 'tp')), parts along dimension 0
There are 2 independent parts, one for each index of `grp`. A program takes and returns all parts, laid end to end along the dimension named above; an argument that names none is the same for every part. Nothing has to cross between parts.
All inputs are finite; a program needn't handle non-finite values.
Results may differ from a plain program's by a relative error of at most 0.024.
Values may be sent and summed in bfloat16 or wider, within the bound.
A program may use at most 128 MiB of HBM per device.

v0:
```python
import jax
import jax.numpy as jnp
from jax import lax
from jax.sharding import PartitionSpec as P

epsilon = 1e-06


def per_device(prompt, norm_gain, up_weight, down_weight):
    folded = (norm_gain[:, None] * up_weight).astype(jnp.bfloat16)
    down_local = down_weight.astype(jnp.bfloat16)
    down_serving = lax.all_gather(down_local, "tp", axis=1, tiled=True)
    thin_rows = lax.all_to_all(folded, "tp", split_axis=0, concat_axis=1, tiled=True)
    crossed = lax.all_to_all(thin_rows, "fs", split_axis=1, concat_axis=0, tiled=True)
    stacked = lax.all_gather(crossed, "tp", axis=0, tiled=True)
    tp_count = lax.axis_size("tp")
    fs_count = lax.axis_size("fs")
    slice_height = folded.shape[0] // tp_count
    unit_count = stacked.shape[1]
    up_serving = stacked.reshape(tp_count, fs_count, slice_height, unit_count)
    up_serving = up_serving.transpose(1, 0, 2, 3).reshape(-1, unit_count)
    widened = prompt.astype(jnp.float32)
    normed = (
        widened * lax.rsqrt(jnp.mean(widened * widened, axis=-1, keepdims=True) + epsilon)
    ).astype(jnp.bfloat16)
    projected = jnp.dot(
        lax.all_gather(normed, "fs", axis=0, tiled=True),
        up_serving,
        preferred_element_type=jnp.float32,
    )
    hidden = jnp.square(jax.nn.relu(projected)).astype(jnp.bfloat16)
    summed = lax.psum_scatter(
        jnp.dot(hidden, down_serving, preferred_element_type=jnp.float32).astype(jnp.bfloat16),
        "fs",
        scatter_dimension=0,
        tiled=True,
    )
    return (up_serving, down_serving, summed)


def solution(mesh):
    return jax.shard_map(
        per_device,
        mesh=mesh,
        in_specs=(P(("grp", "fs", "tp"), None), P("fs"), P("fs", "tp"), P("fs", "tp")),
        out_specs=(P("grp", "fs"), P("fs", "grp"), P(("grp", "fs", "tp"), None)),
        check_vma=False,
    )
```

profile of v0, /device:TPU:0, one launch (start us, length us, event | category | flops | bytes accessed | tf_op | source)
XLA Modules:
  0.0 255.5 jit_solution(17152566268026169703)
XLA Ops:
  7.2 0.0 all-gather.3.cloned.1.call-start
  7.2 2.5 multiply_convert_fusion
  9.7 29.7 %all_to_all.32 = bf16[4,128,2048]{2,1,0:T(8,128)(2,1)S(1)} all-to-all(bf16[4,128,2048]{2,1,0:T(8,128)(2,1)S(1)} %bitcast.17), channel_id=1, replica_groups=mesh['grp'=2,'fs'=4,'tp'=4] {'tp'}, dimensions={0} | all-to-all | bytes 4194304 | tf_op jit(solution)/shard_map/all_to_all | solution.py:13
  39.4 0.0 copy-start
  39.4 52.7 %all_to_all.33 = bf16[128,4,2048]{2,0,1:T(8,128)(2,1)} all-to-all(bf16[128,4,2048]{2,0,1:T(8,128)(2,1)S(1)} %bitcast.16), channel_id=1, replica_groups=mesh['grp'=2,'fs'=4,'tp'=4] {'fs'}, dimensions={1} | all-to-all | bytes 4194304 | tf_op jit(solution)/shard_map/all_to_all | solution.py:14
  92.1 0.0 all-gather.3.cloned.1.call-update
  92.1 0.0 all-gather.5.cloned.1.call-start
  92.2 3.8 %convert_element_type.19 = bf16[2048,512]{1,0:T(8,128)(2,1)} convert(f32[2048,512]{1,0:T(8,128)} %param.7) | non-fusion elementwise | flops 1048576 | bytes 6291456 | tf_op jit(solution)/shard_map/convert_element_type | solution.py:11
  96.0 0.0 all-gather.5.cloned.1.call-update
  96.0 0.0 reduce-scatter.2.cloned.1.call-start
  96.0 0.0 copy-done
  96.1 0.1 fusion.3
  96.2 0.1 fusion.4
  96.3 15.7 %all_gather.11 = bf16[128,2048]{1,0:T(8,128)(2,1)S(1)} all-gather(bf16[32,2048]{1,0:T(8,128)(2,1)S(1)} %fusion.4), channel_id=1, replica_groups=mesh['grp'=2,'fs'=4,'tp'=4] {'fs'}, dimensions={0}, use_global_device_ids=true | all-gather | bytes 655360 | tf_op jit(solution)/shard_map/all_gather | solution.py:27
  112.0 37.2 %all-gather.3.cloned.1.call-done = bf16[2048,2048]{1,0:T(8,128)(2,1)} async-done(((bf16[512,2048]{1,0:T(8,128)(2,1)}), bf16[2048,2048]{1,0:T(8,128)(2,1)}) %all-gather.3.cloned.1.call-update) | async-done | bytes 8388624 | tf_op jit(solution)/shard_map/all_gather | solution.py:15
  149.2 8.4 %copy.7 = bf16[4,4,128,2048]{3,2,1,0:T(8,128)(2,1)} copy(bf16[4,4,128,2048]{3,2,0,1:T(8,128)(2,1)} %bitcast.14) | data formatting | bytes 16777216 | tf_op jit(solution)/shard_map/transpose | solution.py:21
  157.6 52.0 %all-gather.5.cloned.1.call-done = bf16[2048,2048]{1,0:T(8,128)(2,1)} async-done(((bf16[2048,512]{1,0:T(8,128)(2,1)}), bf16[2048,2048]{1,0:T(8,128)(2,1)}) %all-gather.5.cloned.1.call-update) | async-done | bytes 8388624 | tf_op jit(solution)/shard_map/all_gather | solution.py:12
  209.6 8.9 %convolution_convert_fusion = bf16[128,2048]{1,0:T(8,128)(2,1)} fusion(bf16[2048,2048]{1,0:T(8,128)(2,1)} %all-gather.5.cloned.1.call-done, bf16[128,2048]{1,0:T(8,128)(2,1)S(1)} %all_gather.11, bf16[2048,2048]{1,0:T(8,128)(2,1)} %bitcast.12), kind=kOutput, calls=%fused_computation.3 | convolution fusion | flops 2148532224 | bytes 17825792 | tf_op jit(solution)/shard_map/dot_general | solution.py:33
  218.5 0.0 reduce-scatter.2.cloned.1.call-update
  218.5 22.0 %reduce-scatter.2.cloned.1.call-done = bf16[32,2048]{1,0:T(8,128)(2,1)} async-done(((bf16[128,2048]{1,0:T(8,128)(2,1)}), bf16[32,2048]{1,0:T(8,128)(2,1)}) %reduce-scatter.2.cloned.1.call-update) | async-done | bytes 131088 | tf_op jit(solution)/shard_map/reduce_scatter | solution.py:32
  240.5 8.4 %copy.9 = bf16[2048,2048]{1,0:T(8,128)(2,1)} copy(bf16[2048,2048]{1,0:T(8,128)(2,1)} %all-gather.5.cloned.1.call-done) | data formatting | bytes 16777216
  (1 shorter events, 0.0 us)
Async XLA Ops:
  7.2 142.0 %all-gather.3.cloned.1.call-start = ((), (), s32[]{:S(2)}) async-start(), calls=%async_computation.3 | async-start | bytes 10485760 | tf_op jit(solution)/shard_map/all_gather | solution.py:15
  39.4 56.7 %copy-start = (bf16[32,2048]{1,0:T(8,128)(2,1)S(1)}, bf16[32,2048]{1,0:T(8,128)(2,1)}, u32[]{:S(2)}) copy-start(bf16[32,2048]{1,0:T(8,128)(2,1)} %param.4) | copy-start | bytes 393220
  92.1 117.4 %all-gather.5.cloned.1.call-start = ((), (), s32[]{:S(2)}) async-start(), calls=%async_computation.4 | async-start | bytes 10485760 | tf_op jit(solution)/shard_map/all_gather | solution.py:12
  96.0 144.5 %reduce-scatter.2.cloned.1.call-start = ((), (), s32[]{:S(2)}) async-start(), calls=%async_computation.5 | async-start | bytes 655360 | tf_op jit(solution)/shard_map/reduce_scatter | solution.py:32
Sparse Core Ops, SparseCore 0:
  92.3 56.8 all-gather.2
  151.3 58.2 all-gather.4
  218.7 21.8 reduce-scatter.1
where the time goes:
time: 256 us; the launch traced here: 255 us
  waiting for transfers between devices  111 us (43%)
  blocking collectives  98.1 us (38%)
  local copies, waits for them, and re-layouts  16.9 us (7%)
  between operations  13.8 us (5%)
  matrix products  8.93 us (3%)
  other arithmetic  6.49 us (3%)
    all_to_all x1, blocking collectives, per_device(): lax.all_to_all(thin_rows, 'fs', split_axis=1, concat_axis=0, tiled=True)  52.7 us
    all_gather x1, waiting for transfers between devices, per_device(): down_serving = lax.all_gather(down_local, 'tp', axis=1, tiled=True)  52 us
    all_gather x1, waiting for transfers between devices, per_device(): stacked = lax.all_gather(crossed, 'tp', axis=0, tiled=True)  37.2 us
    all_to_all x1, blocking collectives, per_device(): lax.all_to_all(folded, 'tp', split_axis=0, concat_axis=1, tiled=True)  29.7 us
    reduce_scatter x1, waiting for transfers between devices, per_device(): lax.psum_scatter(jnp.dot(hidden, down_serving, preferred_element_type=jnp...  22 us
    all_gather x1, blocking collectives, per_device(): lax.all_gather(normed, 'fs', axis=0, tiled=True)  15.7 us
    dot_general x1, matrix products, per_device(): jnp.dot(hidden, down_serving, preferred_element_type=jnp.float32)  8.93 us
    unnamed x3, local copies, waits for them, and re-layouts  8.44 us
  transfers between devices with their start and end apart: 3, of which 3 were waited for; matrix products, arithmetic and copies ran while one was open for 5% of the time, Pallas kernels for 0%

commit v1 on v0

v1 whole, which is shorter than its diff:
```python
import functools

import jax
import jax.numpy as jnp
from jax import lax
from jax.experimental import pallas as pl
from jax.experimental.pallas import tpu as pltpu
from jax.sharding import PartitionSpec as P

epsilon = 1e-06
CORES = 2
MESH = pl.DeviceIdType.MESH


def kernel(
    groups, fs_count, tp_count, up_steps, down_chunks, down_split,
    ub, db, nb, up_v, down_v, out_v,
    nall, proj, hidden, pbuf, rbuf,
    up_send, up_recv, upf_send, own_send, own_recv,
    dn_send, dn_recv, dnf_send, sib_send, sib_recv,
    n_send, n_recv, r_send, r_recv,
):
    y, z, t = lax.axis_index("grp"), lax.axis_index("fs"), lax.axis_index("tp")
    x, c = t // CORES, lax.rem(t, CORES)
    chips = tp_count // CORES
    ratio, rows, units = ub.shape
    chunk = rows // (up_steps * CORES * groups)
    width = db.shape[1]
    dchunk = units // down_chunks
    tokens = nb.shape[0]
    sibling = (y, z, x * CORES + 1 - c)
    t_src = z // ratio
    x_src, c_src = t_src // CORES, lax.rem(t_src, CORES)
    same_x = x == x_src

    def remote(src, dst, ssem, rsem, dev):
        return pltpu.make_async_remote_copy(
            src_ref=src, dst_ref=dst, send_sem=ssem, recv_sem=rsem, device_id=dev, device_id_type=MESH
        )

    def n_copy(d):
        dst = nall.at[pl.ds(pl.multiple_of(z * tokens, tokens), tokens), :]
        return remote(nb, dst, n_send.at[d], n_recv.at[z], (y, lax.rem(z + d, fs_count), t))

    @pl.loop(1, fs_count)
    def _(d):
        n_copy(d).start()

    def up_at(zr, k):
        return up_v.at[pl.ds(pl.multiple_of(zr * rows + k * chunk, chunk), chunk), :]

    def up_index(m, core, owner):
        return (m * CORES + core) * groups + owner

    def up_first(j, m, cd, dx):
        k = up_index(m, cd, y)
        src = ub.at[j, pl.ds(pl.multiple_of(k * chunk, chunk), chunk), :]
        dev = (y, t * ratio + j, lax.rem(x + dx, chips) * CORES + cd)
        return remote(src, up_at(z, k), up_send.at[j, m, cd, dx], up_recv.at[z, k], dev)

    def up_sends(act):
        for m in range(up_steps):
            for j in range(ratio):
                for cd in range(CORES):
                    for dx in range(1, chips):
                        act(up_first(j, m, cd, dx))

                    @pl.when(t * ratio + j != z)
                    def _():
                        act(up_first(j, m, cd, 0))

    own_j = lax.rem(z, ratio)
    own_rows = pl.ds(pl.multiple_of(z * rows, rows), rows)

    def own_copy():
        return remote(ub.at[own_j], up_v.at[own_rows, :], own_send, own_recv, sibling)

    def sib_copy():
        cols = pl.ds(pl.multiple_of(t * width, width), width)
        return remote(db, down_v.at[:, cols], sib_send, sib_recv, sibling)

    def dn_at(ts, k):
        return down_v.at[
            pl.ds(pl.multiple_of(k * dchunk, dchunk), dchunk), pl.ds(pl.multiple_of(ts * width, width), width)
        ]

    def dn_first(k, dx):
        src = db.at[pl.ds(pl.multiple_of(k * dchunk, dchunk), dchunk), :]
        dev = (y, z, lax.rem(x + dx, chips) * CORES + c)
        return remote(src, dn_at(t, k), dn_send.at[k, dx], dn_recv.at[t, k], dev)

    def dn_sends(act):
        for n in range(down_split):
            for dx in range(1, chips):
                act(dn_first(n * groups + y, dx))
        for k in range(down_split * groups, down_chunks):
            for dx in range(1, chips):
                act(dn_first(k, dx))

    start = lambda copy: copy.start()

    up_sends(start)

    @pl.when(t == t_src)
    def _():
        own_copy().start()

    sib_copy().start()
    dn_sends(start)

    my_cols = pl.ds(pl.multiple_of(t * width, width), width)
    piece = units // down_chunks

    @pl.loop(0, down_chunks)
    def _(i):
        part = pl.ds(pl.multiple_of(i * piece, piece), piece)
        down_v[part, my_cols] = db[part, :]

    @pl.when(t == t_src)
    def _():
        @pl.loop(0, rows // chunk)
        def _(i):
            part = pl.ds(pl.multiple_of(i * chunk, chunk), chunk)
            up_v[pl.ds(pl.multiple_of(z * rows + i * chunk, chunk), chunk), :] = ub[own_j, part, :]

    nall[pl.ds(pl.multiple_of(z * tokens, tokens), tokens), :] = nb[...]

    def up_y(zr, k, g):
        dev = (lax.rem(y + g, groups), z, t)
        return remote(up_at(zr, k), up_at(zr, k), upf_send.at[zr, k, g], up_recv.at[zr, k], dev)

    def up_s(zr, k):
        return remote(up_at(zr, k), up_at(zr, k), upf_send.at[zr, k, 0], up_recv.at[zr, k], sibling)

    def dn_y(ts, k, g):
        dev = (lax.rem(y + g, groups), z, t)
        return remote(dn_at(ts, k), dn_at(ts, k), dnf_send.at[ts, k, g], dn_recv.at[ts, k], dev)

    def dn_s(ts, k):
        return remote(dn_at(ts, k), dn_at(ts, k), dnf_send.at[ts, k, 0], dn_recv.at[ts, k], sibling)

    def if_remote(d, fn):
        if d == 0:
            pl.when(jnp.logical_not(same_x))(fn)
        else:
            fn()

    def up_a(m, d):
        def go():
            zr, k = lax.rem(z + d, fs_count), up_index(m, c, y)
            up_s(zr, k).wait_recv()
            for g in range(1, groups):
                up_y(zr, k, g).start()
            up_s(zr, k).start()

        if_remote(d, go)

    def up_b(m, d):
        def go():
            zr = lax.rem(z + d, fs_count)
            for g in range(1, groups):
                k = up_index(m, c, lax.rem(y + g, groups))
                up_s(zr, k).wait_recv()
                up_s(zr, k).start()

        if_remote(d, go)

    def up_c(d):
        def go():
            zr = lax.rem(z + d, fs_count)
            for m in range(up_steps):
                for owner in range(groups):
                    up_s(zr, up_index(m, 1 - c, owner)).wait_recv()

        if_remote(d, go)

    def up_f(d):
        def go():
            zr = lax.rem(z + d, fs_count)
            for m in range(up_steps):
                for owner in range(groups):
                    up_s(zr, up_index(m, c, owner)).wait_send()
                for g in range(1, groups):
                    up_y(zr, up_index(m, c, y), g).wait_send()

        if_remote(d, go)

    def dn_src(dx):
        return lax.rem(x + dx, chips) * CORES + c

    def dn_a(n, dx):
        ts, k = dn_src(dx), n * groups + y
        dn_s(ts, k).wait_recv()
        for g in range(1, groups):
            dn_y(ts, k, g).start()
        dn_s(ts, k).start()

    def dn_b(n, dx):
        for g in range(1, groups):
            ts, k = dn_src(dx), n * groups + lax.rem(y + g, groups)
            dn_s(ts, k).wait_recv()
            dn_s(ts, k).start()

    def dn_n(k, dx):
        dn_s(dn_src(dx), k).wait_recv()
        dn_s(dn_src(dx), k).start()

    ups = [(m, d) for m in range(up_steps) for d in range(fs_count)]
    lag = fs_count // 2
    for i in range(len(ups) + lag):
        if i < len(ups):
            up_a(*ups[i])
        if i >= lag:
            up_b(*ups[i - lag])
    for n in range(down_split):
        for dx in range(1, chips):
            dn_a(n, dx)

    for d in range(fs_count):
        up_c(d)

    @pl.when(jnp.logical_and(same_x, t != t_src))
    def _():
        own_copy().wait_recv()

    @pl.loop(1, fs_count)
    def _(d):
        zr = lax.rem(z + d, fs_count)
        dst = nall.at[pl.ds(pl.multiple_of(zr * tokens, tokens), tokens), :]
        remote(nb, dst, n_send.at[d], n_recv.at[zr], (y, zr, t)).wait_recv()

    depth = nb.shape[1]
    kb = 256
    nb_tile = min(units, 1024)

    rest = [functools.partial(dn_b, n, dx) for n in range(down_split) for dx in range(1, chips)]
    rest += [
        functools.partial(dn_n, k, dx)
        for k in range(down_split * groups, down_chunks)
        for dx in range(1, chips)
    ]
    pieces = depth // kb
    done = 0
    for i in range(pieces):
        for j in range(units // nb_tile):
            col = pl.ds(j * nb_tile, nb_tile)
            term = jnp.dot(
                nall[:, i * kb : (i + 1) * kb],
                up_v[i * kb : (i + 1) * kb, col],
                preferred_element_type=jnp.float32,
            )
            if i == 0:
                proj[:, col] = term
            else:
                proj[:, col] += term
        upto = len(rest) * (i + 1) // pieces
        for fn in rest[done:upto]:
            fn()
        done = upto

    positive = jnp.maximum(proj[...], 0.0)
    hidden[...] = (positive * positive).astype(jnp.bfloat16)

    def out_copy(ts, d):
        zt = lax.rem(z + d, fs_count)
        cols = pl.ds(pl.multiple_of(ts * width, width), width)
        return remote(pbuf.at[zt, :, cols], rbuf.at[z, :, cols], r_send.at[ts, d], r_recv.at[z, ts], (y, zt, t))

    def block(ts):
        cols = pl.ds(pl.multiple_of(ts * width, width), width)
        part = jnp.dot(hidden[...], down_v[:, cols], preferred_element_type=jnp.float32).astype(jnp.bfloat16)
        pbuf[:, :, cols] = part.reshape(fs_count, tokens, width)

    def send_block(ts):
        @pl.loop(1, fs_count)
        def _(d):
            out_copy(ts, d).start()

    order = [t, x * CORES + 1 - c]
    for dx in range(1, chips):
        order += [dn_src(dx), lax.rem(x + dx, chips) * CORES + 1 - c]
    for i, ts in enumerate(order):
        if i == 1:
            sib_copy().wait_recv()
        if i >= CORES and i % CORES == 1:
            for k in range(down_chunks):
                dn_s(ts, k).wait_recv()
        block(ts)
        if i > 0:
            send_block(order[i - 1])
    send_block(order[-1])

    for d in range(fs_count):
        up_f(d)
    for dx in range(1, chips):
        ts = dn_src(dx)
        for k in range(down_chunks):
            dn_s(ts, k).wait_send()
        for n in range(down_split):
            for g in range(1, groups):
                dn_y(ts, n * groups + y, g).wait_send()
    up_sends(lambda copy: copy.wait_send())
    dn_sends(lambda copy: copy.wait_send())
    sib_copy().wait_send()

    @pl.when(t == t_src)
    def _():
        own_copy().wait_send()

    @pl.loop(1, fs_count)
    def _(d):
        n_copy(d).wait_send()

    total = pbuf[z].astype(jnp.float32)

    @pl.loop(1, fs_count)
    def _(d):
        zr = lax.rem(z + d, fs_count)
        for ts in range(tp_count):
            cols = pl.ds(ts * width, width)
            remote(pbuf.at[zr, :, cols], rbuf.at[zr, :, cols], r_send.at[ts, d], r_recv.at[zr, ts], (y, zr, t)).wait()

    for d in range(1, fs_count):
        total += rbuf[lax.rem(z + d, fs_count)].astype(jnp.float32)
    out_v[...] = total.astype(jnp.bfloat16)


def per_device(groups, prompt, norm_gain, up_weight, down_weight):
    tp_count, fs_count = lax.axis_size("tp"), lax.axis_size("fs")
    rows, wide = up_weight.shape
    units, width = down_weight.shape
    tokens, depth = prompt.shape
    ratio = wide // units
    folded = (norm_gain[:, None] * up_weight).astype(jnp.bfloat16)
    folded = folded.reshape(rows, ratio, units).transpose(1, 0, 2)
    down_local = down_weight.astype(jnp.bfloat16)
    widened = prompt.astype(jnp.float32)
    normed = (
        widened * lax.rsqrt(jnp.mean(widened * widened, axis=-1, keepdims=True) + epsilon)
    ).astype(jnp.bfloat16)
    up_steps = max(1, min(2, rows // (CORES * groups * 16)))
    down_chunks = 8
    down_split = down_chunks // (2 * groups)
    chips = tp_count // CORES
    kc = up_steps * CORES * groups
    dma = pltpu.SemaphoreType.DMA
    vmem = pl.BlockSpec(memory_space=pltpu.VMEM)
    return pl.pallas_call(
        functools.partial(kernel, groups, fs_count, tp_count, up_steps, down_chunks, down_split),
        out_shape=(
            pltpu.VMEM((depth, units), jnp.bfloat16),
            pltpu.VMEM((units, depth), jnp.bfloat16),
            jax.ShapeDtypeStruct((tokens, depth), jnp.bfloat16),
        ),
        in_specs=[vmem] * 3,
        out_specs=(vmem,) * 3,
        scratch_shapes=[
            pltpu.VMEM((fs_count * tokens, depth), jnp.bfloat16),
            pltpu.VMEM((fs_count * tokens, units), jnp.float32),
            pltpu.VMEM((fs_count * tokens, units), jnp.bfloat16),
            pltpu.VMEM((fs_count, tokens, depth), jnp.bfloat16),
            pltpu.VMEM((fs_count, tokens, depth), jnp.bfloat16),
            dma((ratio, up_steps, CORES, chips)),
            dma((fs_count, kc)),
            dma((fs_count, kc, groups)),
            dma, dma,
            dma((down_chunks, chips)),
            dma((tp_count, down_chunks)),
            dma((tp_count, down_chunks, groups)),
            dma, dma,
            dma((fs_count,)),
            dma((fs_count,)),
            dma((tp_count, fs_count)),
            dma((fs_count, tp_count)),
        ],
        compiler_params=pltpu.CompilerParams(has_side_effects=True, vmem_limit_bytes=24 * 1024 * 1024),
    )(folded, down_local, normed)


def solution(mesh):
    return jax.shard_map(
        functools.partial(per_device, mesh.shape["grp"]),
        mesh=mesh,
        in_specs=(P(("grp", "fs", "tp"), None), P("fs"), P("fs", "tp"), P("fs", "tp")),
        out_specs=(P("grp", "fs"), P("fs", "grp"), P(("grp", "fs", "tp"), None)),
        check_vma=False,
    )
```

time: 256 us -> 158 us (0.62)
  Pallas kernels: 0 us -> 143 us
  waiting for transfers between devices: 111 us -> 0 us
  blocking collectives: 98.1 us -> 0 us
  between operations: 13.8 us -> 0.68 us
  local copies, waits for them, and re-layouts: 16.9 us -> 7.45 us
  matrix products: 8.93 us -> 0 us
    pallas_call x0 -> x1, Pallas kernels: none -> 143 us  [per_device(): pl.pallas_call(functools.partial(kernel, groups, fs_count, tp_count, up_s...]
    all_gather x2 -> x0, waiting for transfers between devices: 89.2 us -> none  [the longest x1 52 us: per_device(): down_serving = lax.all_gather(down_local, 'tp', axis=1, tiled=True)]
    all_to_all x2 -> x0, blocking collectives: 82.4 us -> none  [the longest x1 52.7 us: per_device(): lax.all_to_all(thin_rows, 'fs', split_axis=1, concat_axis=0, tiled=True)]
    reduce_scatter x1 -> x0, waiting for transfers between devices: 22 us -> none  [per_device(): lax.psum_scatter(jnp.dot(hidden, down_serving, preferred_element_type=jnp...]
    all_gather x1 -> x0, blocking collectives: 15.7 us -> none  [per_device(): lax.all_gather(normed, 'fs', axis=0, tiled=True)]
    dot_general x1 -> x0, matrix products: 8.93 us -> none  [per_device(): jnp.dot(hidden, down_serving, preferred_element_type=jnp.float32)]
    transpose x1 -> x0, local copies, waits for them, and re-layouts: 8.44 us -> none  [per_device(): up_serving = up_serving.transpose(1, 0, 2, 3).reshape(-1, unit_count)]
    convert_element_type x1, other arithmetic: 3.78 us -> 0.27 us  [per_device(): down_local = down_weight.astype(jnp.bfloat16)]
  transfers between devices with their start and end apart: 3 -> 0, of which waited for: 3 -> 0; matrix products, arithmetic and copies ran while one was open for 5% -> 0% of each run, Pallas kernels for 0% -> 0%
where the time goes in v1:
time: 158 us; the launch traced here: 156 us
  Pallas kernels  143 us (91%)
  local copies, waits for them, and re-layouts  7.45 us (5%)
  other arithmetic  5.05 us (3%)
    pallas_call x1, Pallas kernels, per_device(): pl.pallas_call(functools.partial(kernel, groups, fs_count, tp_count, up_s...  143 us
    unnamed x5, local copies, waits for them, and re-layouts  7.45 us

profile of v1, /device:TPU:0, one launch (start us, length us, event | category | flops | bytes accessed | tf_op | source)
XLA Modules:
  0.0 156.2 jit_solution(15023390305843826436)
XLA Ops:
  0.6 0.0 copy-start
  0.6 1.2 fusion.1
  1.8 1.1 fusion.2.nb
  2.9 2.5 %fusion.ub = bf16[1,512,2048]{2,1,0:T(8,128)(2,1)S(1)} fusion(f32[512,2048]{1,0:T(8,128)} %param.6, f32[512]{0:T(512)} %param.5), kind=kLoop, calls=%fused_computation.1 | loop fusion | flops 2097152 | bytes 6293504 | tf_op jit(solution)/shard_map/transpose;reshape | solution.py:335
  5.4 0.0 copy-done
  5.4 0.3 convert_element_type.13.db
  5.7 143.1 %shard_map.67 = (bf16[2048,2048]{1,0:T(8,128)(2,1)S(1)}, bf16[2048,2048]{1,0:T(8,128)(2,1)S(1)}, bf16[32,2048]{1,0:T(8,128)(2,1)S(1)}) custom-call(bf16[1,512,2048]{2,1,0:T(8,128)(2,1)S(1)} %fusion.ub, bf16[2048,512]{1,0:T(8,128)(2,1)S(1)} %convert_element_type.13.db, bf16[32,2048]{1,0:T(8,128)(2,1)S(1)} %fusion.2.nb), custom_call_target="tpu_custom_call" | custom-call | tf_op jit(solution)/shard_map/pallas_call | solution.py:348
  148.8 3.4 %copy.10 = bf16[2048,2048]{1,0:T(8,128)(2,1)} copy(bf16[2048,2048]{1,0:T(8,128)(2,1)S(1)} %get-tuple-element.3) | data formatting | bytes 16777216
  152.2 3.4 %copy.11 = bf16[2048,2048]{1,0:T(8,128)(2,1)} copy(bf16[2048,2048]{1,0:T(8,128)(2,1)S(1)} %get-tuple-element.4) | data formatting | bytes 16777216
  155.6 0.7 copy.12
  (1 shorter events, 0.0 us)
Async XLA Ops:
  0.6 4.8 %copy-start = (f32[2048,512]{1,0:T(8,128)S(1)}, f32[2048,512]{1,0:T(8,128)}, u32[]{:S(2)}) copy-start(f32[2048,512]{1,0:T(8,128)} %param.7) | copy-start | bytes 12582916

commit v2 on v1

--- a/solution.py
+++ b/solution.py
@@ -9,14 +9,15 @@
 
 epsilon = 1e-06
 CORES = 2
+UP_STEPS = 4
 MESH = pl.DeviceIdType.MESH
 
 
 def kernel(
     groups, fs_count, tp_count, up_steps, down_chunks, down_split,
     ub, db, nb, up_v, down_v, out_v,
-    nall, proj, hidden, pbuf, rbuf,
-    up_send, up_recv, upf_send, own_send, own_recv,
+    nall, proj, hidden, pbuf, rbuf, stage,
+    up_send, stage_recv, z_send, up_recv, upf_send, own_send, own_recv,
     dn_send, dn_recv, dnf_send, sib_send, sib_recv,
     n_send, n_recv, r_send, r_recv,
 ):
@@ -52,22 +53,54 @@
     def up_index(m, core, owner):
         return (m * CORES + core) * groups + owner
 
-    def up_first(j, m, cd, dx):
+    def src_at(j, m, cd):
         k = up_index(m, cd, y)
-        src = ub.at[j, pl.ds(pl.multiple_of(k * chunk, chunk), chunk), :]
-        dev = (y, t * ratio + j, lax.rem(x + dx, chips) * CORES + cd)
-        return remote(src, up_at(z, k), up_send.at[j, m, cd, dx], up_recv.at[z, k], dev)
-
-    def up_sends(act):
+        return ub.at[j, pl.ds(pl.multiple_of(k * chunk, chunk), chunk), :]
+
+    def up_x(j, m, cd, dx):
+        dev = (y, z, lax.rem(x + dx, chips) * CORES + c)
+        sem = up_send.at[j, m, cd, dx]
+        return remote(src_at(j, m, cd), stage.at[x, j, m, cd], sem, stage_recv.at[x, j, m, cd], dev)
+
+    def up_x_own(j, m, cd, dx):
+        dev = (y, z, lax.rem(x + dx, chips) * CORES + cd)
+        k = up_index(m, cd, y)
+        return remote(src_at(j, m, cd), up_at(z, k), up_send.at[j, m, cd, dx], up_recv.at[z, k], dev)
+
+    def up_x_all(act):
         for m in range(up_steps):
-            for j in range(ratio):
-                for cd in range(CORES):
+            for cd in range(CORES):
+                for j in range(ratio):
+                    mine = t * ratio + j == z
                     for dx in range(1, chips):
-                        act(up_first(j, m, cd, dx))
-
-                    @pl.when(t * ratio + j != z)
-                    def _():
-                        act(up_first(j, m, cd, 0))
+                        @pl.when(mine)
+                        def _():
+                            act(up_x_own(j, m, cd, dx))
+
+                        @pl.when(jnp.logical_not(mine))
+                        def _():
+                            act(up_x(j, m, cd, dx))
+
+    def up_z(j, m, cd, dx):
+        xs = lax.rem(x + dx, chips)
+        src = src_at(j, m, cd) if dx == 0 else stage.at[xs, j, m, cd]
+        k = up_index(m, cd, y)
+        dev = (y, (xs * CORES + c) * ratio + j, x * CORES + cd)
+        return remote(src, up_at(z, k), z_send.at[j, m, cd, dx], up_recv.at[z, k], dev)
+
+    def up_z_one(j, m, cd, dx, act):
+        xs = lax.rem(x + dx, chips)
+
+        @pl.when((xs * CORES + c) * ratio + j != z)
+        def _():
+            act(j, m, cd, dx)
+
+    def go_z(j, m, cd, dx):
+        if dx > 0:
+            xs = lax.rem(x + dx, chips)
+            at = stage.at[xs, j, m, cd]
+            remote(at, at, up_send.at[j, m, cd, dx], stage_recv.at[xs, j, m, cd], sibling).wait_recv()
+        up_z(j, m, cd, dx).start()
 
     own_j = lax.rem(z, ratio)
     own_rows = pl.ds(pl.multiple_of(z * rows, rows), rows)
@@ -99,7 +132,11 @@
 
     start = lambda copy: copy.start()
 
-    up_sends(start)
+    for m in range(1):
+        for cd in range(CORES):
+            for j in range(ratio):
+                up_z_one(j, m, cd, 0, go_z)
+    up_x_all(start)
 
     @pl.when(t == t_src)
     def _():
@@ -205,13 +242,20 @@
         dn_s(dn_src(dx), k).wait_recv()
         dn_s(dn_src(dx), k).start()
 
-    ups = [(m, d) for m in range(up_steps) for d in range(fs_count)]
-    lag = fs_count // 2
-    for i in range(len(ups) + lag):
-        if i < len(ups):
-            up_a(*ups[i])
-        if i >= lag:
-            up_b(*ups[i - lag])
+    for m in range(up_steps + 2):
+        if m < up_steps:
+            for cd in range(CORES):
+                for j in range(ratio):
+                    if m + 1 < up_steps:
+                        up_z_one(j, m + 1, cd, 0, go_z)
+                    for dx in range(1, chips):
+                        up_z_one(j, m, cd, dx, go_z)
+        if 1 <= m <= up_steps:
+            for d in range(fs_count):
+                up_a(m - 1, d)
+        if m >= 2:
+            for d in range(fs_count):
+                up_b(m - 2, d)
     for n in range(down_split):
         for dx in range(1, chips):
             dn_a(n, dx)
@@ -299,7 +343,12 @@
         for n in range(down_split):
             for g in range(1, groups):
                 dn_y(ts, n * groups + y, g).wait_send()
-    up_sends(lambda copy: copy.wait_send())
+    up_x_all(lambda copy: copy.wait_send())
+    for m in range(up_steps):
+        for cd in range(CORES):
+            for j in range(ratio):
+                for dx in range(chips):
+                    up_z_one(j, m, cd, dx, lambda *at: up_z(*at).wait_send())
     dn_sends(lambda copy: copy.wait_send())
     sib_copy().wait_send()
 
@@ -338,7 +387,7 @@
     normed = (
         widened * lax.rsqrt(jnp.mean(widened * widened, axis=-1, keepdims=True) + epsilon)
     ).astype(jnp.bfloat16)
-    up_steps = max(1, min(2, rows // (CORES * groups * 16)))
+    up_steps = max(1, min(UP_STEPS, rows // (CORES * groups * 16)))
     down_chunks = 8
     down_split = down_chunks // (2 * groups)
     chips = tp_count // CORES
@@ -360,6 +409,9 @@
             pltpu.VMEM((fs_count * tokens, units), jnp.bfloat16),
             pltpu.VMEM((fs_count, tokens, depth), jnp.bfloat16),
             pltpu.VMEM((fs_count, tokens, depth), jnp.bfloat16),
+            pltpu.VMEM((chips, ratio, up_steps, CORES, rows // kc, units), jnp.bfloat16),
+            dma((ratio, up_steps, CORES, chips)),
+            dma((chips, ratio, up_steps, CORES)),
             dma((ratio, up_steps, CORES, chips)),
             dma((fs_count, kc)),
             dma((fs_count, kc, groups)),

time: 158 us -> 121 us (0.77)
  Pallas kernels: 143 us -> 106 us
    pallas_call x1, Pallas kernels: 143 us -> 106 us  [per_device(): pl.pallas_call(functools.partial(kernel, groups, fs_count, tp_count, up_s...]
where the time goes in v2:
time: 121 us; the launch traced here: 119 us
  Pallas kernels  106 us (88%)
  local copies, waits for them, and re-layouts  7.45 us (6%)
  other arithmetic  5.05 us (4%)
    pallas_call x1, Pallas kernels, per_device(): pl.pallas_call(functools.partial(kernel, groups, fs_count, tp_count, up_s...  106 us
    unnamed x5, local copies, waits for them, and re-layouts  7.45 us
    another operation x1, other arithmetic, per_device(): folded = folded.reshape(rows, ratio, units).transpose(1, 0, 2)  2.47 us

profile of v2, /device:TPU:0, one launch (start us, length us, event | category | flops | bytes accessed | tf_op | source)
XLA Modules:
  0.0 119.5 jit_solution(11249725504126983259)
XLA Ops:
  0.6 0.0 copy-start
  0.6 1.2 fusion.1
  1.8 1.1 fusion.2.nb
  2.9 2.5 %fusion.ub = bf16[1,512,2048]{2,1,0:T(8,128)(2,1)S(1)} fusion(f32[512,2048]{1,0:T(8,128)} %param.6, f32[512]{0:T(512)} %param.5), kind=kLoop, calls=%fused_computation.1 | loop fusion | flops 2097152 | bytes 6293504 | tf_op jit(solution)/shard_map/transpose;reshape | solution.py:384
  5.4 0.0 copy-done
  5.4 0.3 convert_element_type.13.db
  5.7 106.3 %shard_map.67 = (bf16[2048,2048]{1,0:T(8,128)(2,1)S(1)}, bf16[2048,2048]{1,0:T(8,128)(2,1)S(1)}, bf16[32,2048]{1,0:T(8,128)(2,1)S(1)}) custom-call(bf16[1,512,2048]{2,1,0:T(8,128)(2,1)S(1)} %fusion.ub, bf16[2048,512]{1,0:T(8,128)(2,1)S(1)} %convert_element_type.13.db, bf16[32,2048]{1,0:T(8,128)(2,1)S(1)} %fusion.2.nb), custom_call_target="tpu_custom_call" | custom-call | tf_op jit(solution)/shard_map/pallas_call | solution.py:397
  112.0 3.4 %copy.10 = bf16[2048,2048]{1,0:T(8,128)(2,1)} copy(bf16[2048,2048]{1,0:T(8,128)(2,1)S(1)} %get-tuple-element.3) | data formatting | bytes 16777216
  115.4 3.4 %copy.11 = bf16[2048,2048]{1,0:T(8,128)(2,1)} copy(bf16[2048,2048]{1,0:T(8,128)(2,1)S(1)} %get-tuple-element.4) | data formatting | bytes 16777216
  118.8 0.7 copy.12
  (1 shorter events, 0.0 us)
Async XLA Ops:
  0.6 4.8 %copy-start = (f32[2048,512]{1,0:T(8,128)S(1)}, f32[2048,512]{1,0:T(8,128)}, u32[]{:S(2)}) copy-start(f32[2048,512]{1,0:T(8,128)} %param.7) | copy-start | bytes 12582916

commit v3 on v2

--- a/solution.py
+++ b/solution.py
@@ -10,6 +10,9 @@
 epsilon = 1e-06
 CORES = 2
 UP_STEPS = 4
+DOWN_SPLIT = 0
+LAG_A = 1
+LAG_B = 3
 MESH = pl.DeviceIdType.MESH
 
 
@@ -145,23 +148,6 @@
     sib_copy().start()
     dn_sends(start)
 
-    my_cols = pl.ds(pl.multiple_of(t * width, width), width)
-    piece = units // down_chunks
-
-    @pl.loop(0, down_chunks)
-    def _(i):
-        part = pl.ds(pl.multiple_of(i * piece, piece), piece)
-        down_v[part, my_cols] = db[part, :]
-
-    @pl.when(t == t_src)
-    def _():
-        @pl.loop(0, rows // chunk)
-        def _(i):
-            part = pl.ds(pl.multiple_of(i * chunk, chunk), chunk)
-            up_v[pl.ds(pl.multiple_of(z * rows + i * chunk, chunk), chunk), :] = ub[own_j, part, :]
-
-    nall[pl.ds(pl.multiple_of(z * tokens, tokens), tokens), :] = nb[...]
-
     def up_y(zr, k, g):
         dev = (lax.rem(y + g, groups), z, t)
         return remote(up_at(zr, k), up_at(zr, k), upf_send.at[zr, k, g], up_recv.at[zr, k], dev)
@@ -242,7 +228,7 @@
         dn_s(dn_src(dx), k).wait_recv()
         dn_s(dn_src(dx), k).start()
 
-    for m in range(up_steps + 2):
+    for m in range(up_steps + LAG_B):
         if m < up_steps:
             for cd in range(CORES):
                 for j in range(ratio):
@@ -250,15 +236,32 @@
                         up_z_one(j, m + 1, cd, 0, go_z)
                     for dx in range(1, chips):
                         up_z_one(j, m, cd, dx, go_z)
-        if 1 <= m <= up_steps:
+        if LAG_A <= m < up_steps + LAG_A:
             for d in range(fs_count):
-                up_a(m - 1, d)
-        if m >= 2:
+                up_a(m - LAG_A, d)
+        if m >= LAG_B:
             for d in range(fs_count):
-                up_b(m - 2, d)
+                up_b(m - LAG_B, d)
     for n in range(down_split):
         for dx in range(1, chips):
             dn_a(n, dx)
+
+    my_cols = pl.ds(pl.multiple_of(t * width, width), width)
+    piece = units // down_chunks
+
+    @pl.loop(0, down_chunks)
+    def _(i):
+        part = pl.ds(pl.multiple_of(i * piece, piece), piece)
+        down_v[part, my_cols] = db[part, :]
+
+    @pl.when(t == t_src)
+    def _():
+        @pl.loop(0, rows // chunk)
+        def _(i):
+            part = pl.ds(pl.multiple_of(i * chunk, chunk), chunk)
+            up_v[pl.ds(pl.multiple_of(z * rows + i * chunk, chunk), chunk), :] = ub[own_j, part, :]
+
+    nall[pl.ds(pl.multiple_of(z * tokens, tokens), tokens), :] = nb[...]
 
     for d in range(fs_count):
         up_c(d)
@@ -389,7 +392,7 @@
     ).astype(jnp.bfloat16)
     up_steps = max(1, min(UP_STEPS, rows // (CORES * groups * 16)))
     down_chunks = 8
-    down_split = down_chunks // (2 * groups)
+    down_split = DOWN_SPLIT
     chips = tp_count // CORES
     kc = up_steps * CORES * groups
     dma = pltpu.SemaphoreType.DMA

time: 121 us -> 111 us (0.917)
  Pallas kernels: 106 us -> 96.1 us
    pallas_call x1, Pallas kernels: 106 us -> 96.1 us  [per_device(): pl.pallas_call(functools.partial(kernel, groups, fs_count, tp_count, up_s...]
where the time goes in v3:
time: 111 us; the launch traced here: 109 us
  Pallas kernels  96.1 us (87%)
  local copies, waits for them, and re-layouts  7.45 us (7%)
  other arithmetic  5.05 us (5%)
    pallas_call x1, Pallas kernels, per_device(): pl.pallas_call(functools.partial(kernel, groups, fs_count, tp_count, up_s...  96.1 us
    unnamed x5, local copies, waits for them, and re-layouts  7.45 us
    another operation x1, other arithmetic, per_device(): folded = folded.reshape(rows, ratio, units).transpose(1, 0, 2)  2.47 us

profile of v3, /device:TPU:0, one launch (start us, length us, event | category | flops | bytes accessed | tf_op | source)
XLA Modules:
  0.0 109.2 jit_solution(3283178022704422882)
XLA Ops:
  0.6 0.0 copy-start
  0.6 1.2 %fusion.1 = f32[32]{0:T(128)S(1)} fusion(bf16[32,2048]{1,0:T(8,128)(2,1)} %param.4), kind=kLoop, calls=%fused_computation.4 | loop fusion | flops 196576 | bytes 131200 | tf_op jit(solution)/shard_map/reduce_sum | solution.py:391
  1.8 1.1 %fusion.2.nb = bf16[32,2048]{1,0:T(8,128)(2,1)S(1)} fusion(bf16[32,2048]{1,0:T(8,128)(2,1)} %param.4, f32[32]{0:T(128)S(1)} %add_rsqrt_fusion), kind=kLoop, calls=%fused_computation.5 | loop fusion | flops 196608 | bytes 262272 | tf_op jit(solution)/shard_map/convert_element_type | solution.py:392
  2.9 2.5 %fusion.ub = bf16[1,512,2048]{2,1,0:T(8,128)(2,1)S(1)} fusion(f32[512,2048]{1,0:T(8,128)} %param.6, f32[512]{0:T(512)} %param.5), kind=kLoop, calls=%fused_computation.1 | loop fusion | flops 2097152 | bytes 6293504 | tf_op jit(solution)/shard_map/transpose;reshape | solution.py:387
  5.4 0.0 copy-done
  5.4 0.3 convert_element_type.13.db
  5.7 96.1 %shard_map.67 = (bf16[2048,2048]{1,0:T(8,128)(2,1)S(1)}, bf16[2048,2048]{1,0:T(8,128)(2,1)S(1)}, bf16[32,2048]{1,0:T(8,128)(2,1)S(1)}) custom-call(bf16[1,512,2048]{2,1,0:T(8,128)(2,1)S(1)} %fusion.ub, bf16[2048,512]{1,0:T(8,128)(2,1)S(1)} %convert_element_type.13.db, bf16[32,2048]{1,0:T(8,128)(2,1)S(1)} %fusion.2.nb), custom_call_target="tpu_custom_call" | custom-call | tf_op jit(solution)/shard_map/pallas_call | solution.py:400
  101.8 3.4 %copy.10 = bf16[2048,2048]{1,0:T(8,128)(2,1)} copy(bf16[2048,2048]{1,0:T(8,128)(2,1)S(1)} %get-tuple-element.3) | data formatting | bytes 16777216
  105.2 3.4 %copy.11 = bf16[2048,2048]{1,0:T(8,128)(2,1)} copy(bf16[2048,2048]{1,0:T(8,128)(2,1)S(1)} %get-tuple-element.4) | data formatting | bytes 16777216
  108.6 0.7 copy.12
  (1 shorter events, 0.0 us)
Async XLA Ops:
  0.6 4.8 %copy-start = (f32[2048,512]{1,0:T(8,128)S(1)}, f32[2048,512]{1,0:T(8,128)}, u32[]{:S(2)}) copy-start(f32[2048,512]{1,0:T(8,128)} %param.7) | copy-start | bytes 12582916

commit v4 on v3

--- a/solution.py
+++ b/solution.py
@@ -9,6 +9,7 @@
 
 epsilon = 1e-06
 CORES = 2
+PIECES = 4
 UP_STEPS = 4
 DOWN_SPLIT = 0
 LAG_A = 1
@@ -18,8 +19,8 @@
 
 def kernel(
     groups, fs_count, tp_count, up_steps, down_chunks, down_split,
-    ub, db, nb, up_v, down_v, out_v,
-    nall, proj, hidden, pbuf, rbuf, stage,
+    ub, db, prompt, up_v, down_v, out_v,
+    nb, nall, proj, hidden, pbuf, rbuf, stage,
     up_send, stage_recv, z_send, up_recv, upf_send, own_send, own_recv,
     dn_send, dn_recv, dnf_send, sib_send, sib_recv,
     n_send, n_recv, r_send, r_recv,
@@ -31,7 +32,7 @@
     chunk = rows // (up_steps * CORES * groups)
     width = db.shape[1]
     dchunk = units // down_chunks
-    tokens = nb.shape[0]
+    tokens = prompt.shape[0]
     sibling = (y, z, x * CORES + 1 - c)
     t_src = z // ratio
     x_src, c_src = t_src // CORES, lax.rem(t_src, CORES)
@@ -45,10 +46,6 @@
     def n_copy(d):
         dst = nall.at[pl.ds(pl.multiple_of(z * tokens, tokens), tokens), :]
         return remote(nb, dst, n_send.at[d], n_recv.at[z], (y, lax.rem(z + d, fs_count), t))
-
-    @pl.loop(1, fs_count)
-    def _(d):
-        n_copy(d).start()
 
     def up_at(zr, k):
         return up_v.at[pl.ds(pl.multiple_of(zr * rows + k * chunk, chunk), chunk), :]
@@ -147,6 +144,10 @@
 
     sib_copy().start()
     dn_sends(start)
+
+    widened = prompt[...].astype(jnp.float32)
+    scale = lax.rsqrt(jnp.mean(widened * widened, axis=-1, keepdims=True) + epsilon)
+    nb[...] = (widened * scale).astype(jnp.bfloat16)
 
     def up_y(zr, k, g):
         dev = (lax.rem(y + g, groups), z, t)
@@ -263,6 +264,10 @@
 
     nall[pl.ds(pl.multiple_of(z * tokens, tokens), tokens), :] = nb[...]
 
+    @pl.loop(1, fs_count)
+    def _(d):
+        n_copy(d).start()
+
     for d in range(fs_count):
         up_c(d)
 
@@ -276,7 +281,7 @@
         dst = nall.at[pl.ds(pl.multiple_of(zr * tokens, tokens), tokens), :]
         remote(nb, dst, n_send.at[d], n_recv.at[zr], (y, zr, t)).wait_recv()
 
-    depth = nb.shape[1]
+    depth = prompt.shape[1]
     kb = 256
     nb_tile = min(units, 1024)
 
@@ -377,6 +382,19 @@
     out_v[...] = total.astype(jnp.bfloat16)
 
 
+def write_out(up_v, down_v, out_v, up_out, down_out, mlp_out, sems):
+    copies = [pltpu.make_async_copy(out_v, mlp_out, sems.at[2 * PIECES])]
+    for n, (src, dst) in enumerate(((up_v, up_out), (down_v, down_out))):
+        step = src.shape[0] // PIECES
+        for i in range(PIECES):
+            part = pl.ds(i * step, step)
+            copies.append(pltpu.make_async_copy(src.at[part, :], dst.at[part, :], sems.at[n * PIECES + i]))
+    for copy in copies:
+        copy.start()
+    for copy in copies:
+        copy.wait()
+
+
 def per_device(groups, prompt, norm_gain, up_weight, down_weight):
     tp_count, fs_count = lax.axis_size("tp"), lax.axis_size("fs")
     rows, wide = up_weight.shape
@@ -386,10 +404,6 @@
     folded = (norm_gain[:, None] * up_weight).astype(jnp.bfloat16)
     folded = folded.reshape(rows, ratio, units).transpose(1, 0, 2)
     down_local = down_weight.astype(jnp.bfloat16)
-    widened = prompt.astype(jnp.float32)
-    normed = (
-        widened * lax.rsqrt(jnp.mean(widened * widened, axis=-1, keepdims=True) + epsilon)
-    ).astype(jnp.bfloat16)
     up_steps = max(1, min(UP_STEPS, rows // (CORES * groups * 16)))
     down_chunks = 8
     down_split = DOWN_SPLIT
@@ -397,7 +411,7 @@
     kc = up_steps * CORES * groups
     dma = pltpu.SemaphoreType.DMA
     vmem = pl.BlockSpec(memory_space=pltpu.VMEM)
-    return pl.pallas_call(
+    up_v, down_v, out_v = pl.pallas_call(
         functools.partial(kernel, groups, fs_count, tp_count, up_steps, down_chunks, down_split),
         out_shape=(
             pltpu.VMEM((depth, units), jnp.bfloat16),
@@ -407,6 +421,7 @@
         in_specs=[vmem] * 3,
         out_specs=(vmem,) * 3,
         scratch_shapes=[
+            pltpu.VMEM((tokens, depth), jnp.bfloat16),
             pltpu.VMEM((fs_count * tokens, depth), jnp.bfloat16),
             pltpu.VMEM((fs_count * tokens, units), jnp.float32),
             pltpu.VMEM((fs_count * tokens, units), jnp.bfloat16),
@@ -429,7 +444,21 @@
             dma((fs_count, tp_count)),
         ],
         compiler_params=pltpu.CompilerParams(has_side_effects=True, vmem_limit_bytes=24 * 1024 * 1024),
-    )(folded, down_local, normed)
+    )(folded, down_local, prompt)
+    any_space = pl.BlockSpec(memory_space=pl.ANY)
+    return pl.pallas_call(
+        write_out,
+        out_shape=(
+            jax.ShapeDtypeStruct(up_v.shape, jnp.bfloat16),
+            jax.ShapeDtypeStruct(down_v.shape, jnp.bfloat16),
+            jax.ShapeDtypeStruct(out_v.shape, jnp.bfloat16),
+        ),
+        in_specs=[vmem] * 3,
+        out_specs=(any_space,) * 3,
+        scratch_shapes=[dma((2 * PIECES + 1,))],
+        compiler_params=pltpu.CompilerParams(vmem_limit_bytes=1024 * 1024),
+        cost_estimate=pl.CostEstimate(flops=0, bytes_accessed=4 * depth * units * 2, transcendentals=0),
+    )(up_v, down_v, out_v)
 
 
 def solution(mesh):

time: 111 us -> 108 us (0.973); the launches traced: 109 us -> 107 us
  local copies, waits for them, and re-layouts: 7.45 us -> 1.46 us
  Pallas kernels: 96.1 us -> 102 us
  other arithmetic: 5.05 us -> 2.89 us
    unnamed x5 -> x4, local copies, waits for them, and re-layouts: 7.45 us -> 1.46 us
    pallas_call x0 -> x1, Pallas kernels: none -> 5.98 us  [per_device(): pl.pallas_call(write_out, out_shape=(jax.ShapeDtypeStruct(up_v.shape, jnp...]
    reduce_sum x1 -> x0, other arithmetic: 1.19 us -> none  [per_device(): jnp.mean(widened * widened, axis=-1, keepdims=True) + epsilon]
where the time goes in v4:
time: 108 us; the launch traced here: 107 us
  Pallas kernels  102 us (94%)
  other arithmetic  2.89 us (3%)
  local copies, waits for them, and re-layouts  1.46 us (1%)
    pallas_call x1, Pallas kernels, per_device(): pl.pallas_call(functools.partial(kernel, groups, fs_count, tp_count, up_s...  96.4 us
    pallas_call x1, Pallas kernels, per_device(): pl.pallas_call(write_out, out_shape=(jax.ShapeDtypeStruct(up_v.shape, jnp...  5.98 us
    another operation x1, other arithmetic, per_device(): folded = folded.reshape(rows, ratio, units).transpose(1, 0, 2)  2.62 us

profile of v4, /device:TPU:0, one launch (start us, length us, event | category | flops | bytes accessed | tf_op | source)
XLA Modules:
  0.0 107.4 jit_solution(15901315902133850073)
XLA Ops:
  0.6 0.0 copy-start.1
  0.6 2.6 %fusion.ub = bf16[1,512,2048]{2,1,0:T(8,128)(2,1)S(1)} fusion(f32[512,2048]{1,0:T(8,128)} %param.6, f32[512]{0:T(512)} %param.5), kind=kLoop, calls=%fused_computation.1 | loop fusion | flops 2097152 | bytes 6293504 | tf_op jit(solution)/shard_map/transpose;reshape | solution.py:405
  3.3 0.8 copy-done.1
  4.1 0.0 copy-start
  4.1 0.3 convert_element_type.7.db
  4.4 0.6 copy-done
  5.0 96.4 %shard_map.67 = (bf16[2048,2048]{1,0:T(8,128)(2,1)S(1)}, bf16[2048,2048]{1,0:T(8,128)(2,1)S(1)}, bf16[32,2048]{1,0:T(8,128)(2,1)S(1)}) custom-call(bf16[1,512,2048]{2,1,0:T(8,128)(2,1)S(1)} %fusion.ub, bf16[2048,512]{1,0:T(8,128)(2,1)S(1)} %convert_element_type.7.db, bf16[32,2048]{1,0:T(8,128)(2,1)S(1)} %copy-done), custom_call_target="tpu_custom_call" | custom-call | tf_op jit(solution)/shard_map/pallas_call | solution.py:414
  101.4 6.0 %shard_map.68 = (bf16[2048,2048]{1,0:T(8,128)(2,1)}, bf16[2048,2048]{1,0:T(8,128)(2,1)}, bf16[32,2048]{1,0:T(8,128)(2,1)}) custom-call(bf16[2048,2048]{1,0:T(8,128)(2,1)S(1)} %get-tuple-element.6.up_v, bf16[2048,2048]{1,0:T(8,128)(2,1)S(1)} %get-tuple-element.7.down_v, bf16[32,2048]{1,0:T(8,128)(2,1)S(1)} %get-tuple-element.8.out_v), custom_call_target="tpu_custom_call" | custom-call | bytes 33554432 | tf_op jit(solution)/shard_map/pallas_call | solution.py:449
Async XLA Ops:
  0.6 3.5 %copy-start.1 = (f32[2048,512]{1,0:T(8,128)S(1)}, f32[2048,512]{1,0:T(8,128)}, u32[]{:S(2)}) copy-start(f32[2048,512]{1,0:T(8,128)} %param.7) | copy-start | bytes 12582916
  4.1 0.9 copy-start
